TPU v7x, 32 devices: a whole 2x2x4 slice. The times are simulated.
32 devices in a mesh: sp: 4 (over z), fs: 4 (over y, x), tp: 2 (over core).
Axes of the slice: x: 2, y: 2, z: 4, core: 2. Of those that a mesh axis runs over, the one named last changes fastest.
Arguments:
- tokens: bfloat16 [4096, 2048], P(('fs', 'sp')), parts along dimension 0, may hold values from -6 to 6
- norm_gain: float32 [2048], replicated, may hold values from 0.1 to 1.9
- w_query: bfloat16 [2048, 1024], P('sp', 'tp'), may hold values from -0.080939698 to 0.080939698
- w_key: bfloat16 [2048, 256], P('sp', 'tp'), may hold values from -0.080939698 to 0.080939698
- w_value: bfloat16 [2048, 256], P('sp', 'tp'), may hold values from -0.125 to 0.125
- w_conv_in: bfloat16 [2048, 1024], P('sp', 'tp'), may hold values from -0.125 to 0.125
- w_conv_gate: bfloat16 [2048, 1024], P('sp', 'tp'), may hold values from -0.125 to 0.125
- sink_logit: float32 [16], P('tp'), may hold values from 2 to 6
- conv_taps: float32 [31, 1024], P(None, 'tp'), may hold values from -5.3881591 to 5.3881591
- conv_bias: float32 [1024], P('tp'), may hold values from -0.9 to 5.9
- channel_gain: float32 [1024], P('tp'), may hold values from 0.1 to 1.9
- channel_shift: float32 [1024], P('tp'), may hold values from -3 to 3
- w_attn_out: bfloat16 [1024, 2048], P(None, 'sp'), may hold values from -1.5 to 1.5
- w_conv_out: bfloat16 [1024, 2048], P(None, 'sp'), may hold values from -0.1875 to 0.1875
Outputs:
- output: bfloat16 [4096, 2048], P(('fs', 'sp', 'tp')), parts along dimension 0
There are 4 independent parts, one for each index of `fs`. A program takes and returns all parts, laid end to end along the dimension named above; an argument that names none is the same for every part. Nothing has to cross between parts.
All inputs are finite; a program needn't handle non-finite values.
Results may differ from a plain program's by a relative error of at most 0.011.
Values may be sent and summed in bfloat16 or wider, within the bound.
A program may use at most 64 MiB of HBM per device.

v0:
```python
import jax
import jax.numpy as jnp
from jax import lax
from jax.sharding import PartitionSpec as P

HEAD_DIM = 64
WINDOW = 128
GRID_W = 64
EPSILON = 1e-06
NEGATIVE = -1e30
ROPE_BASE = 10000.0


def padded(block, sides, width):
    for axis, dim in sides:
        count = lax.axis_size(axis)
        forward = [(i, i + 1) for i in range(count - 1)]
        backward = [(target, source) for source, target in forward]
        low = lax.ppermute(
            lax.slice_in_dim(block, block.shape[dim] - width, None, axis=dim), axis, forward
        )
        high = lax.ppermute(lax.slice_in_dim(block, 0, width, axis=dim), axis, backward)
        block = jnp.concatenate([low, block, high], axis=dim)
    return block


def rotate_pairs(values, positions):
    middle = values.shape[-1] // 2
    inverse = ROPE_BASE ** (-jnp.arange(middle, dtype=jnp.float32) / middle)
    angles = positions.astype(jnp.float32)[:, None] * inverse[None, :]
    cosine = jnp.cos(angles)[:, None, :]
    sine_table = jnp.sin(angles)[:, None, :]
    leading = values[..., :middle]
    trailing = values[..., middle:]
    return jnp.concatenate(
        [leading * cosine - trailing * sine_table, leading * sine_table + trailing * cosine],
        axis=-1,
    )


def grid_rotate(values, positions):
    middle = values.shape[-1] // 2
    return jnp.concatenate(
        [
            rotate_pairs(values[..., :middle], positions // GRID_W),
            rotate_pairs(values[..., middle:], positions % GRID_W),
        ],
        axis=-1,
    )


def local(
    tokens,
    norm_gain,
    w_query,
    w_key,
    w_value,
    w_conv_in,
    w_conv_gate,
    sink_logit,
    conv_taps,
    conv_bias,
    channel_gain,
    channel_shift,
    w_attn_out,
    w_conv_out,
):
    rows_here = tokens.shape[0]
    offset = lax.axis_index("sp") * rows_here
    total = rows_here * lax.axis_size("sp")
    tp_count = lax.axis_size("tp")
    token_float = tokens.astype(jnp.float32)
    normed = (
        token_float
        * lax.rsqrt(jnp.mean(token_float * token_float, axis=-1, keepdims=True) + EPSILON)
        * norm_gain[None, :]
    ).astype(jnp.bfloat16)
    head_cols = w_query.shape[1]
    kv_cols = w_key.shape[1]
    chan_cols = w_conv_in.shape[1]
    piece_query = lax.all_gather(w_query, "sp", axis=0, tiled=True)
    piece_key = lax.all_gather(w_key, "sp", axis=0, tiled=True)
    piece_value = lax.all_gather(w_value, "sp", axis=0, tiled=True)
    piece_conv = lax.all_gather(w_conv_in, "sp", axis=0, tiled=True)
    piece_gate = lax.all_gather(w_conv_gate, "sp", axis=0, tiled=True)
    query_acc = jnp.dot(normed, piece_query, preferred_element_type=jnp.float32)
    pair_acc = jnp.dot(
        normed,
        jnp.concatenate([piece_key, piece_value], axis=1),
        preferred_element_type=jnp.float32,
    )
    conv_acc = jnp.dot(
        normed,
        jnp.concatenate([piece_conv, piece_gate], axis=1),
        preferred_element_type=jnp.float32,
    )
    positions = offset + jnp.arange(rows_here, dtype=jnp.int32)
    heads_here = head_cols // HEAD_DIM
    kv_here = kv_cols // HEAD_DIM
    group = heads_here // kv_here
    query = grid_rotate(query_acc.reshape(rows_here, heads_here, HEAD_DIM), positions).astype(
        jnp.bfloat16
    )
    keys = grid_rotate(pair_acc[:, :kv_cols].reshape(rows_here, kv_here, HEAD_DIM), positions)
    keys = keys.astype(jnp.bfloat16).reshape(rows_here, kv_cols)
    values = pair_acc[:, kv_cols:].astype(jnp.bfloat16)
    stacked = jnp.concatenate([keys, values], axis=1)
    extended = padded(stacked, (("sp", 0),), WINDOW)
    block = min(rows_here, 512)
    span = block + 2 * WINDOW
    sinks = sink_logit.reshape(kv_here, group)[:, :, None, None]
    queries = query.reshape(block, kv_here, group, HEAD_DIM)
    near_keys = extended[:, :kv_cols].reshape(span, kv_here, HEAD_DIM)
    near_values = extended[:, kv_cols:].reshape(span, kv_here, HEAD_DIM)
    scores = jnp.einsum(
        "qkgd,skd->kgqs", queries, near_keys, preferred_element_type=jnp.float32
    ) * HEAD_DIM ** (-0.5)
    query_pos = offset + 0 + jnp.arange(block, dtype=jnp.int32)
    key_pos = offset + 0 - WINDOW + jnp.arange(span, dtype=jnp.int32)
    valid = (
        (jnp.abs(query_pos[:, None] - key_pos[None, :]) <= WINDOW)
        & (key_pos[None, :] >= 0)
        & (key_pos[None, :] < total)
    )
    scores = jnp.where(valid[None, None], scores, NEGATIVE)
    top = jnp.maximum(jnp.max(scores, axis=-1, keepdims=True), sinks)
    raised = jnp.exp(scores - top)
    denominator = jnp.sum(raised, axis=-1, keepdims=True) + jnp.exp(sinks - top)
    probs = (raised / denominator).astype(jnp.bfloat16)
    mixed = jnp.einsum("kgqs,skd->qkgd", probs, near_values, preferred_element_type=jnp.float32)
    outputs = mixed.astype(jnp.bfloat16).reshape(block, head_cols)
    glu = (conv_acc[:, :chan_cols] * jax.nn.sigmoid(conv_acc[:, chan_cols:])).astype(jnp.bfloat16)
    reach = conv_taps.shape[0] // 2
    rims = padded(glu, (("sp", 0),), reach)
    filtered = jnp.zeros((rows_here, chan_cols), jnp.float32) + conv_bias[None, :]
    for shift_index in range(conv_taps.shape[0]):
        filtered = filtered + conv_taps[shift_index][None, :] * rims[
            shift_index : shift_index + rows_here
        ].astype(jnp.float32)
    channel_total = chan_cols * tp_count
    centre = lax.psum(jnp.sum(filtered, axis=-1), "tp")[:, None] / channel_total
    centred = filtered - centre
    spread = lax.psum(jnp.sum(centred * centred, axis=-1), "tp")[:, None] / channel_total
    conv_out = jax.nn.silu(
        centred * lax.rsqrt(spread + EPSILON) * channel_gain[None, :] + channel_shift[None, :]
    ).astype(jnp.bfloat16)
    features = jnp.concatenate([outputs, conv_out], axis=1)
    tp_here = lax.axis_index("tp")
    own_rows = jnp.concatenate(
        [
            lax.dynamic_slice_in_dim(w_attn_out, tp_here * head_cols, head_cols, 0),
            lax.dynamic_slice_in_dim(w_conv_out, tp_here * chan_cols, chan_cols, 0),
        ],
        axis=0,
    )
    own_whole = lax.all_gather(own_rows, "sp", axis=1, tiled=True)
    result = lax.psum_scatter(
        jnp.dot(features, own_whole, preferred_element_type=jnp.float32).astype(jnp.bfloat16),
        "tp",
        scatter_dimension=0,
        tiled=True,
    )
    return result


def solution(mesh):
    in_specs = (
        P(("fs", "sp"), None),
        P(),
        P("sp", "tp"),
        P("sp", "tp"),
        P("sp", "tp"),
        P("sp", "tp"),
        P("sp", "tp"),
        P("tp"),
        P(None, "tp"),
        P("tp"),
        P("tp"),
        P("tp"),
        P(None, "sp"),
        P(None, "sp"),
    )
    out_specs = P(("fs", "sp", "tp"), None)
    return jax.shard_map(local, mesh=mesh, in_specs=in_specs, out_specs=out_specs, check_vma=False)
```

profile of v0, /device:TPU:0, one launch (start us, length us, event | category | flops | bytes accessed | tf_op | source)
XLA Modules:
  0.0 263.5 jit_solution(13735289390232705822)
XLA Ops:
  6.5 0.7 all-gather.7.cloned.1.call-update
  7.3 0.7 all-gather.9.cloned.1.call-update
  8.1 0.7 all-gather.5.cloned.1.call-update
  8.8 1.3 constant_dynamic-slice_fusion
  10.1 1.0 pad_maximum_fusion
  11.3 0.3 fusion.6
  11.6 23.1 %all_gather.18 = bf16[2048,128]{1,0:T(8,128)(2,1)S(1)} all-gather(bf16[512,128]{1,0:T(8,128)(2,1)S(1)} %copy-done.1), channel_id=1, replica_groups=mesh['sp'=4,'fs'=4,'tp'=2] {'sp'}, dimensions={0}, use_global_device_ids=true | all-gather | bytes 655360 | tf_op jit(solution)/shard_map/all_gather | solution.py:82
  34.7 21.7 %all_gather.19 = bf16[2048,128]{1,0:T(8,128)(2,1)S(1)} all-gather(bf16[512,128]{1,0:T(8,128)(2,1)S(1)} %copy-done.2), channel_id=1, replica_groups=mesh['sp'=4,'fs'=4,'tp'=2] {'sp'}, dimensions={0}, use_global_device_ids=true | all-gather | bytes 655360 | tf_op jit(solution)/shard_map/all_gather | solution.py:83
  56.4 0.7 fusion.11
  57.4 1.5 collective-permute-start
  58.9 1.3 collective-permute-start.1
  60.3 0.3 fusion.24
  60.7 1.5 collective-permute-done
  62.2 7.0 %collective-permute-done.1 = bf16[128,256]{0,1:T(8,128)(2,1)S(1)} collective-permute-done((bf16[128,256]{0,1:T(8,128)(2,1)S(1)}, bf16[128,256]{0,1:T(8,128)(2,1)S(1)}, u32[]{:S(2)}, u32[]{:S(2)}) %collective-permute-start.1) | collective-permute-done | bytes 65568 | tf_op jit(solution)/shard_map/ppermute | solution.py:22
  69.2 1.9 all-gather.7.cloned.1.call-done
  71.1 47.3 %all-gather.9.cloned.1.call-done = bf16[2048,512]{1,0:T(8,128)(2,1)} async-done(((bf16[512,512]{1,0:T(8,128)(2,1)}), bf16[2048,512]{1,0:T(8,128)(2,1)}) %all-gather.9.cloned.1.call-update) | async-done | bytes 2097168 | tf_op jit(solution)/shard_map/all_gather | solution.py:85
  118.4 3.5 %fusion = f32[256,1024]{1,0:T(8,128)S(1)} fusion(bf16[2048,512]{1,0:T(8,128)(2,1)} %all-gather.9.cloned.1.call-done, bf16[2048,512]{1,0:T(8,128)(2,1)} %all-gather.7.cloned.1.call-done, bf16[256,2048]{1,0:T(8,128)(2,1)S(1)} %copy-done, f32[2048]{0:T(1024)S(1)} %copy-done.7, f32[256]{0:T(256)S(1)} %add_rsqrt_fusion.1), kind=kOutput, calls=%fused_computation | convolution fusion | flops 1084227584 | bytes 6300672 | tf_op jit(solution)/shard_map/dot_general | solution.py:92
  122.1 2.1 collective-permute-start.2
  124.2 1.3 collective-permute-start.3
  125.5 39.2 %all-gather.5.cloned.1.call-done = bf16[2048,512]{1,0:T(8,128)(2,1)} async-done(((bf16[512,512]{1,0:T(8,128)(2,1)}), bf16[2048,512]{1,0:T(8,128)(2,1)}) %all-gather.5.cloned.1.call-update) | async-done | bytes 2097168 | tf_op jit(solution)/shard_map/all_gather | solution.py:81
  164.6 2.6 fusion.74
  167.3 0.8 fusion.5
  168.2 0.9 fusion.4
  169.3 1.2 fusion.10
  170.7 3.1 %fusion.77 = (f32[256]{0:T(256)S(1)}, f32[256,512]{1,0:T(8,128)S(1)}) fusion(bf16[15,512]{1,0:T(8,128)(2,1)S(1)} %collective-permute-done.3, bf16[256,512]{1,0:T(8,128)(2,1)S(1)} %fusion.22, f32[512]{0:T(512)S(1)} %bitcast.106, f32[512]{0:T(512)S(1)} %bitcast.107, f32[512]{0:T(512)S(1)} %bitcast.78, f32[512]{0:T(512)S(1)} %bitcast.79, f32[512]{0:T(512)S(1)} %bitcast.80, ...), kind=kLoop, calls=%fused_computation.167 | loop fusion | flops 24116992 | bytes 883712 | tf_op jit(solution)/shard_map/reduce_sum | solution.py:141
  173.8 2.5 psum.14
  176.2 0.2 multiply_reduce_fusion
  176.4 2.5 psum.15
  178.9 0.3 multiply_convert_fusion
  179.2 66.3 %all-gather.11.cloned.1.call-done = bf16[1024,2048]{1,0:T(8,128)(2,1)} async-done(((bf16[1024,512]{1,0:T(8,128)(2,1)}), bf16[1024,2048]{1,0:T(8,128)(2,1)}) %all-gather.11.cloned.1.call-update) | async-done | bytes 4194320 | tf_op jit(solution)/shard_map/all_gather | solution.py:156
  245.5 4.5 %convolution_convert_fusion = bf16[256,2048]{1,0:T(8,128)(2,1)} fusion(bf16[1024,2048]{1,0:T(8,128)(2,1)} %all-gather.11.cloned.1.call-done, bf16[256,512]{1,0:T(8,128)(2,1)S(1)} %multiply_convert_fusion, bf16[256,512]{1,0:T(8,128)(2,1)S(1)} %copy.27), kind=kOutput, calls=%fused_computation.11 | convolution fusion | flops 1075314688 | bytes 5767168 | tf_op jit(solution)/shard_map/dot_general | solution.py:158
  249.9 7.0 %reduce-scatter.2.cloned.1.call-done = bf16[128,2048]{1,0:T(8,128)(2,1)} async-done(((bf16[256,2048]{1,0:T(8,128)(2,1)}), bf16[128,2048]{1,0:T(8,128)(2,1)}) %reduce-scatter.2.cloned.1.call-update) | async-done | bytes 524304 | tf_op jit(solution)/shard_map/reduce_scatter | solution.py:157
  (52 shorter events, 1.3 us)
Async XLA Ops:
  6.5 4.7 %copy-start = (bf16[256,2048]{1,0:T(8,128)(2,1)S(1)}, bf16[256,2048]{1,0:T(8,128)(2,1)}, u32[]{:S(2)}) copy-start(bf16[256,2048]{1,0:T(8,128)(2,1)} %param.14) | copy-start | bytes 3145732
  6.5 5.0 %copy-start.1 = (bf16[512,128]{1,0:T(8,128)(2,1)S(1)}, bf16[512,128]{1,0:T(8,128)(2,1)}, u32[]{:S(2)}) copy-start(bf16[512,128]{1,0:T(8,128)(2,1)} %param.17) | copy-start | bytes 393220
  6.5 28.1 %copy-start.2 = (bf16[512,128]{1,0:T(8,128)(2,1)S(1)}, bf16[512,128]{1,0:T(8,128)(2,1)}, u32[]{:S(2)}) copy-start(bf16[512,128]{1,0:T(8,128)(2,1)} %param.18) | copy-start | bytes 393220
  6.5 64.6 %all-gather.7.cloned.1.call-start = ((), (), s32[]{:S(2)}) async-start(), calls=%async_computation.2 | async-start | bytes 2621440 | tf_op jit(solution)/shard_map/all_gather | solution.py:84
  7.3 111.1 %all-gather.9.cloned.1.call-start = ((), (), s32[]{:S(2)}) async-start(), calls=%async_computation.3 | async-start | bytes 2621440 | tf_op jit(solution)/shard_map/all_gather | solution.py:85
  8.0 48.4 %copy-start.7 = (f32[2048]{0:T(1024)S(1)}, f32[2048]{0:T(1024)}, u32[]{:S(2)}) copy-start(f32[2048]{0:T(1024)} %param.15) | copy-start | bytes 24580
  8.0 156.6 %all-gather.5.cloned.1.call-start = ((), (), s32[]{:S(2)}) async-start(), calls=%async_computation.1 | async-start | bytes 2621440 | tf_op jit(solution)/shard_map/all_gather | solution.py:81
  8.8 236.7 %all-gather.11.cloned.1.call-start = ((), (), s32[]{:S(2)}) async-start(), calls=%async_computation.4 | async-start | bytes 5242880 | tf_op jit(solution)/shard_map/all_gather | solution.py:156
  11.1 49.1 %copy-start.3 = (f32[31,512]{1,0:T(8,128)S(1)}, f32[31,512]{1,0:T(8,128)}, u32[]{:S(2)}) copy-start(f32[31,512]{1,0:T(8,128)} %param.22) | copy-start | bytes 190468
  11.1 49.5 %copy-start.8 = (f32[8]{0:T(128)S(1)}, f32[8]{0:T(128)}, u32[]{:S(2)}) copy-start(f32[8]{0:T(128)} %param.21) | copy-start | bytes 100
  11.2 245.8 %reduce-scatter.2.cloned.1.call-start = ((), (), s32[]{:S(2)}) async-start(), calls=%async_computation.5 | async-start | bytes 1572864 | tf_op jit(solution)/shard_map/reduce_scatter | solution.py:157
  57.4 4.8 %collective-permute-start = (bf16[128,256]{0,1:T(8,128)(2,1)S(1)}, bf16[128,256]{0,1:T(8,128)(2,1)S(1)}, u32[]{:S(2)}, u32[]{:S(2)}) collective-permute-start(bf16[128,256]{0,1:T(8,128)(2,1)S(1)} %get-tuple-element.21), channel_id=1, source_target_pairs={{0,8},{8,16},{16,24},{1,9},{9,17},{17,25},{2,10},{10,18},{18,26},{... | collective-permute-start | bytes 196616 | tf_op jit(solution)/shard_map/ppermute | solution.py:19
  58.9 10.3 %collective-permute-start.1 = (bf16[128,256]{0,1:T(8,128)(2,1)S(1)}, bf16[128,256]{0,1:T(8,128)(2,1)S(1)}, u32[]{:S(2)}, u32[]{:S(2)}) collective-permute-start(bf16[128,256]{0,1:T(8,128)(2,1)S(1)} %get-tuple-element.22), channel_id=1, source_target_pairs={{8,0},{16,8},{24,16},{9,1},{17,9},{25,17},{10,2},{18,10},{26,18},{... | collective-permute-start | bytes 196616 | tf_op jit(solution)/shard_map/ppermute | solution.py:22
  122.1 48.6 %collective-permute-start.2 = (bf16[15,512]{1,0:T(8,128)(2,1)S(1)}, bf16[15,512]{1,0:T(8,128)(2,1)S(1)}, u32[]{:S(2)}, u32[]{:S(2)}) collective-permute-start(bf16[15,512]{1,0:T(8,128)(2,1)S(1)} %get-tuple-element.15), channel_id=1, source_target_pairs={{0,8},{8,16},{16,24},{1,9},{9,17},{17,25},{2,10},{10,18},{18,26},{... | collective-permute-start | bytes 46088 | tf_op jit(solution)/shard_map/ppermute | solution.py:19
  124.2 46.5 %collective-permute-start.3 = (bf16[15,512]{1,0:T(8,128)(2,1)S(1)}, bf16[15,512]{1,0:T(8,128)(2,1)S(1)}, u32[]{:S(2)}, u32[]{:S(2)}) collective-permute-start(bf16[15,512]{1,0:T(8,128)(2,1)S(1)} %get-tuple-element.16), channel_id=1, source_target_pairs={{8,0},{16,8},{24,16},{9,1},{17,9},{25,17},{10,2},{18,10},{26,18},{... | collective-permute-start | bytes 46088 | tf_op jit(solution)/shard_map/ppermute | solution.py:22
  169.2 1.4 copy-start.4
  169.2 9.7 %copy-start.5 = (f32[512]{0:T(512)S(1)}, f32[512]{0:T(512)}, u32[]{:S(2)}) copy-start(f32[512]{0:T(512)} %param.25) | copy-start | bytes 6148
  169.2 9.7 %copy-start.6 = (f32[512]{0:T(512)S(1)}, f32[512]{0:T(512)}, u32[]{:S(2)}) copy-start(f32[512]{0:T(512)} %param.24) | copy-start | bytes 6148
Sparse Core Ops, SparseCore 0:
  8.9 62.1 all-gather.6
  72.7 45.6 all-gather.8
  120.0 44.6 all-gather.4
  166.1 79.3 all-gather.10
  250.1 6.8 reduce-scatter.1
where the time goes:
time: 264 us
  waiting for transfers between devices  172 us (65%)
  blocking collectives  49.7 us (19%)
  between operations  13.5 us (5%)
  matrix products  13.3 us (5%)
  other arithmetic  6.78 us (3%)
  starting transfers between devices  6.35 us (2%)
    all_gather x1, waiting for transfers between devices, local(): own_whole = lax.all_gather(own_rows, 'sp', axis=1, tiled=True)  66.3 us
    all_gather x1, waiting for transfers between devices, local(): piece_gate = lax.all_gather(w_conv_gate, 'sp', axis=0, tiled=True)  47.3 us
    all_gather x1, waiting for transfers between devices, local(): piece_query = lax.all_gather(w_query, 'sp', axis=0, tiled=True)  39.2 us
    all_gather x1, blocking collectives, local(): piece_key = lax.all_gather(w_key, 'sp', axis=0, tiled=True)  23.1 us
    all_gather x1, blocking collectives, local(): piece_value = lax.all_gather(w_value, 'sp', axis=0, tiled=True)  21.7 us
    reduce_scatter x1, waiting for transfers between devices, local(): lax.psum_scatter(jnp.dot(features, own_whole, preferred_element_type=jnp....  7.04 us
    ppermute x2, waiting for transfers between devices, padded(): lax.ppermute(lax.slice_in_dim(block, 0, width, axis=dim), axis, backward)  6.99 us
  transfers between devices with their start and end apart: 9, of which 7 were waited for; matrix products, arithmetic and copies ran while one was open for 7% of the time, Pallas kernels for 0%

commit v1 on v0

--- a/solution.py
+++ b/solution.py
@@ -9,6 +9,23 @@
 EPSILON = 1e-06
 NEGATIVE = -1e30
 ROPE_BASE = 10000.0
+
+
+def classes_fill(arr_in, ax_name):
+    axis_len = lax.axis_size(ax_name)
+    crops = []
+    for nth in range(axis_len):
+        crops.append((nth, (nth + 1) % axis_len))
+
+    def lift_samples(lower):
+        if len(lower) == axis_len:
+            return lower
+        v1 = lift_samples([lax.ppermute(lower[0], axis_name=ax_name, perm=crops), *lower])
+        return v1
+
+    outcome_arr = jnp.concatenate(lift_samples([arr_in]), 0)
+    k_now = jnp.roll(outcome_arr, (lax.axis_index(ax_name) + 1) * arr_in.shape[0], 0)
+    return k_now
 
 
 def padded(block, sides, width):
@@ -78,7 +95,7 @@
     head_cols = w_query.shape[1]
     kv_cols = w_key.shape[1]
     chan_cols = w_conv_in.shape[1]
-    piece_query = lax.all_gather(w_query, "sp", axis=0, tiled=True)
+    piece_query = classes_fill(w_query, "sp")
     piece_key = lax.all_gather(w_key, "sp", axis=0, tiled=True)
     piece_value = lax.all_gather(w_value, "sp", axis=0, tiled=True)
     piece_conv = lax.all_gather(w_conv_in, "sp", axis=0, tiled=True)

time: 264 us -> 235 us (0.89)
  waiting for transfers between devices: 172 us -> 108 us
  starting transfers between devices: 6.35 us -> 21.7 us
  blocking collectives: 49.7 us -> 63 us
  local copies, waits for them, and re-layouts: 1.64 us -> 6.3 us
    all_gather x1, waiting for transfers between devices: 47.3 us -> 3.7 us  [local(): piece_gate = lax.all_gather(w_conv_gate, 'sp', axis=0, tiled=True)]
    all_gather x1 -> x0, waiting for transfers between devices: 39.2 us -> none  [local(): piece_query = lax.all_gather(w_query, 'sp', axis=0, tiled=True)]
    ppermute x0 -> x3, waiting for transfers between devices: none -> 36 us  [lift_samples(): lax.ppermute(lower[0], axis_name=ax_name, perm=crops)]
    all_gather x1, blocking collectives: 23.1 us -> 37.8 us  [local(): piece_key = lax.all_gather(w_key, 'sp', axis=0, tiled=True)]
    all_gather x1, waiting for transfers between devices: 66.3 us -> 53.4 us  [local(): own_whole = lax.all_gather(own_rows, 'sp', axis=1, tiled=True)]
    ppermute x0 -> x3, starting transfers between devices: none -> 9.96 us  [lift_samples(): lax.ppermute(lower[0], axis_name=ax_name, perm=crops)]
    ppermute x2, starting transfers between devices: 3.61 us -> 9.02 us  [padded(): lax.ppermute(lax.slice_in_dim(block, block.shape[dim] - width, None, axis...]
  transfers between devices with their start and end apart: 9 -> 11, of which waited for: 7 -> 6; matrix products, arithmetic and copies ran while one was open for 7% -> 9% of each run, Pallas kernels for 0% -> 0%
where the time goes in v1:
time: 235 us
  waiting for transfers between devices  108 us (46%)
  blocking collectives  63 us (27%)
  starting transfers between devices  21.7 us (9%)
  between operations  14 us (6%)
  matrix products  13.1 us (6%)
  other arithmetic  8.83 us (4%)
  local copies, waits for them, and re-layouts  6.3 us (3%)
    all_gather x1, waiting for transfers between devices, local(): own_whole = lax.all_gather(own_rows, 'sp', axis=1, tiled=True)  53.4 us
    all_gather x1, blocking collectives, local(): piece_key = lax.all_gather(w_key, 'sp', axis=0, tiled=True)  37.8 us
    ppermute x3, waiting for transfers between devices, lift_samples(): lax.ppermute(lower[0], axis_name=ax_name, perm=crops)  36 us
    all_gather x1, blocking collectives, local(): piece_value = lax.all_gather(w_value, 'sp', axis=0, tiled=True)  20.3 us
    ppermute x3, starting transfers between devices, lift_samples(): lax.ppermute(lower[0], axis_name=ax_name, perm=crops)  9.96 us
    ppermute x2, starting transfers between devices, padded(): lax.ppermute(lax.slice_in_dim(block, block.shape[dim] - width, None, axis...  9.02 us
    reduce_scatter x1, waiting for transfers between devices, local(): lax.psum_scatter(jnp.dot(features, own_whole, preferred_element_type=jnp....  7.01 us
    ppermute x2, waiting for transfers between devices, padded(): lax.ppermute(lax.slice_in_dim(block, 0, width, axis=dim), axis, backward)  6.09 us
  transfers between devices with their start and end apart: 11, of which 6 were waited for; matrix products, arithmetic and copies ran while one was open for 9% of the time, Pallas kernels for 0%

profile of v1, /device:TPU:0, one launch (start us, length us, event | category | flops | bytes accessed | tf_op | source)
XLA Modules:
  0.0 234.7 jit_solution(8461513362667270436)
XLA Ops:
  6.5 0.7 all-gather.4.cloned.1.call-update
  8.1 3.1 %collective-permute-start.2 = (bf16[512,512]{1,0:T(8,128)(2,1)}, bf16[512,512]{1,0:T(8,128)(2,1)S(1)}, u32[]{:S(2)}, u32[]{:S(2)}) collective-permute-start(bf16[512,512]{1,0:T(8,128)(2,1)} %param.16), channel_id=1, source_target_pairs={{0,8},{8,16},{16,24},{24,0},{1,9},{9,17},{17,25},{25,1},{2,10},{10... | collective-permute-start | bytes 1572872 | tf_op jit(solution)/shard_map/ppermute | solution.py:23
  11.2 1.5 fusion.6
  12.7 37.8 %all_gather.15 = bf16[2048,128]{1,0:T(8,128)(2,1)S(1)} all-gather(bf16[512,128]{1,0:T(8,128)(2,1)} %param.17), channel_id=1, replica_groups=mesh['sp'=4,'fs'=4,'tp'=2] {'sp'}, dimensions={0}, use_global_device_ids=true | all-gather | bytes 655360 | tf_op jit(solution)/shard_map/all_gather | solution.py:99
  50.5 20.3 %all_gather.16 = bf16[2048,128]{1,0:T(8,128)(2,1)S(1)} all-gather(bf16[512,128]{1,0:T(8,128)(2,1)} %param.18), channel_id=1, replica_groups=mesh['sp'=4,'fs'=4,'tp'=2] {'sp'}, dimensions={0}, use_global_device_ids=true | all-gather | bytes 655360 | tf_op jit(solution)/shard_map/all_gather | solution.py:100
  70.8 1.9 fusion.13
  73.1 3.0 %collective-permute-start = (bf16[128,256]{0,1:T(8,128)(2,1)S(1)}, bf16[128,256]{0,1:T(8,128)(2,1)S(1)}, u32[]{:S(2)}, u32[]{:S(2)}) collective-permute-start(bf16[128,256]{0,1:T(8,128)(2,1)S(1)} %get-tuple-element.21), channel_id=1, source_target_pairs={{0,8},{8,16},{16,24},{1,9},{9,17},{17,25},{2,10},{10,18},{18,26},{... | collective-permute-start | bytes 196616 | tf_op jit(solution)/shard_map/ppermute | solution.py:36
  76.0 1.3 collective-permute-start.1
  77.4 1.0 pad_maximum_fusion
  78.6 2.7 %collective-permute-start.3 = (bf16[512,512]{1,0:T(8,128)(2,1)S(1)}, bf16[512,512]{1,0:T(8,128)(2,1)S(1)}, u32[]{:S(2)}, u32[]{:S(2)}) collective-permute-start(bf16[512,512]{1,0:T(8,128)(2,1)S(1)} %collective-permute-done.2), channel_id=1, source_target_pairs={{0,8},{8,16},{16,24},{24,0},{1,9},{9,17},{17,25},{25,1},{2,10},{10... | collective-permute-start | bytes 1572872 | tf_op jit(solution)/shard_map/ppermute | solution.py:23
  82.2 17.0 %collective-permute-done.3 = bf16[512,512]{1,0:T(8,128)(2,1)S(1)} collective-permute-done((bf16[512,512]{1,0:T(8,128)(2,1)S(1)}, bf16[512,512]{1,0:T(8,128)(2,1)S(1)}, u32[]{:S(2)}, u32[]{:S(2)}) %collective-permute-start.3) | collective-permute-done | bytes 524320 | tf_op jit(solution)/shard_map/ppermute | solution.py:23
  99.3 4.2 %collective-permute-start.4 = (bf16[512,512]{1,0:T(8,128)(2,1)S(1)}, bf16[512,512]{1,0:T(8,128)(2,1)S(1)}, u32[]{:S(2)}, u32[]{:S(2)}) collective-permute-start(bf16[512,512]{1,0:T(8,128)(2,1)S(1)} %collective-permute-done.3), channel_id=1, source_target_pairs={{0,8},{8,16},{16,24},{24,0},{1,9},{9,17},{17,25},{25,1},{2,10},{10... | collective-permute-start | bytes 1572872 | tf_op jit(solution)/shard_map/ppermute | solution.py:23
  103.4 1.7 fusion.83
  105.1 1.3 max.18
  106.4 0.9 pad_maximum_fusion.3
  107.4 18.9 %collective-permute-done.4 = bf16[512,512]{1,0:T(8,128)(2,1)S(1)} collective-permute-done((bf16[512,512]{1,0:T(8,128)(2,1)S(1)}, bf16[512,512]{1,0:T(8,128)(2,1)S(1)}, u32[]{:S(2)}, u32[]{:S(2)}) %collective-permute-start.4) | collective-permute-done | bytes 524320 | tf_op jit(solution)/shard_map/ppermute | solution.py:23
  126.7 1.1 fusion.9
  127.9 0.8 fusion.5
  128.8 1.9 copy-done
  130.7 0.9 fusion.4
  131.7 3.7 %all-gather.6.cloned.1.call-done = bf16[2048,512]{1,0:T(8,128)(2,1)} async-done(((bf16[512,512]{1,0:T(8,128)(2,1)}), bf16[2048,512]{1,0:T(8,128)(2,1)}) %all-gather.6.cloned.1.call-update) | async-done | bytes 2097168 | tf_op jit(solution)/shard_map/all_gather | solution.py:102
  135.4 3.7 %fusion = f32[256,1024]{1,0:T(8,128)S(1)} fusion(bf16[2048,512]{1,0:T(8,128)(2,1)} %all-gather.6.cloned.1.call-done, bf16[2048,512]{1,0:T(8,128)(2,1)} %all-gather.4.cloned.1.call-done, bf16[256,2048]{1,0:T(8,128)(2,1)S(1)} %copy-done.3, f32[2048]{0:T(1024)S(1)} %copy-done.42, f32[256]{0:T(256)S(1)} %copy-done.40), kind=kOutput, calls=%fused_computation | convolution fusion | flops 1084227584 | bytes 6300672 | tf_op jit(solution)/shard_map/dot_general | solution.py:109
  139.3 6.1 %collective-permute-start.5 = (bf16[15,512]{1,0:T(8,128)(2,1)S(1)}, bf16[15,512]{1,0:T(8,128)(2,1)S(1)}, u32[]{:S(2)}, u32[]{:S(2)}) collective-permute-start(bf16[15,512]{1,0:T(8,128)(2,1)S(1)} %get-tuple-element.15), channel_id=1, source_target_pairs={{0,8},{8,16},{16,24},{1,9},{9,17},{17,25},{2,10},{10,18},{18,26},{... | collective-permute-start | bytes 46088 | tf_op jit(solution)/shard_map/ppermute | solution.py:36
  145.3 1.3 collective-permute-start.6
  146.9 1.2 fusion.12
  148.3 6.1 %collective-permute-done.6 = bf16[15,512]{1,0:T(8,128)(2,1)S(1)} collective-permute-done((bf16[15,512]{1,0:T(8,128)(2,1)S(1)}, bf16[15,512]{1,0:T(8,128)(2,1)S(1)}, u32[]{:S(2)}, u32[]{:S(2)}) %collective-permute-start.6) | collective-permute-done | bytes 15392 | tf_op jit(solution)/shard_map/ppermute | solution.py:39
  154.7 3.1 %fusion.79 = (f32[256]{0:T(256)S(1)}, f32[256,512]{1,0:T(8,128)S(1)}) fusion(bf16[15,512]{1,0:T(8,128)(2,1)S(1)} %collective-permute-done.6, bf16[256,512]{1,0:T(8,128)(2,1)S(1)} %fusion.24, f32[512]{0:T(512)S(1)} %bitcast.105, f32[512]{0:T(512)S(1)} %bitcast.106, f32[512]{0:T(512)S(1)} %bitcast.77, f32[512]{0:T(512)S(1)} %bitcast.78, f32[512]{0:T(512)S(1)} %bitcast.79, ...), kind=kLoop, calls=%fused_computation.177 | loop fusion | flops 24116992 | bytes 883712 | tf_op jit(solution)/shard_map/reduce_sum | solution.py:158
  157.8 2.5 %psum.14 = f32[256]{0:T(256)S(1)} all-reduce(f32[256]{0:T(256)S(1)} %get-tuple-element.5), channel_id=1, replica_groups=mesh['sp'=4,'fs'=4,'tp'=2] {'tp'}, use_global_device_ids=true, to_apply=%region_4.5 | all-reduce | flops 256 | bytes 2048 | tf_op jit(solution)/shard_map/psum | solution.py:158
  160.5 2.5 %psum.15 = f32[256]{0:T(256)S(1)} all-reduce(f32[256]{0:T(256)S(1)} %multiply_reduce_fusion), channel_id=1, replica_groups=mesh['sp'=4,'fs'=4,'tp'=2] {'tp'}, use_global_device_ids=true, to_apply=%region_6.7 | all-reduce | flops 256 | bytes 2048 | tf_op jit(solution)/shard_map/psum | solution.py:160
  163.2 53.4 %all-gather.8.cloned.1.call-done = bf16[1024,2048]{1,0:T(8,128)(2,1)} async-done(((bf16[1024,512]{1,0:T(8,128)(2,1)}), bf16[1024,2048]{1,0:T(8,128)(2,1)}) %all-gather.8.cloned.1.call-update) | async-done | bytes 4194320 | tf_op jit(solution)/shard_map/all_gather | solution.py:173
  216.6 4.4 %convolution_convert_fusion = bf16[256,2048]{1,0:T(8,128)(2,1)} fusion(bf16[1024,2048]{1,0:T(8,128)(2,1)} %all-gather.8.cloned.1.call-done, bf16[256,512]{1,0:T(8,128)(2,1)S(1)} %multiply_convert_fusion, bf16[256,512]{1,0:T(8,128)(2,1)S(1)} %copy.27), kind=kOutput, calls=%fused_computation.11 | convolution fusion | flops 1075314688 | bytes 5767168 | tf_op jit(solution)/shard_map/dot_general | solution.py:175
  221.1 7.0 %reduce-scatter.2.cloned.1.call-done = bf16[128,2048]{1,0:T(8,128)(2,1)} async-done(((bf16[256,2048]{1,0:T(8,128)(2,1)}), bf16[128,2048]{1,0:T(8,128)(2,1)}) %reduce-scatter.2.cloned.1.call-update) | async-done | bytes 524304 | tf_op jit(solution)/shard_map/reduce_scatter | solution.py:174
  (131 shorter events, 3.7 us)
Async XLA Ops:
  6.5 70.8 %copy-start.5 = (bf16[1024,512]{1,0:T(8,128)(2,1)S(1)}, bf16[1024,512]{1,0:T(8,128)(2,1)}, u32[]{:S(2)}) copy-start(bf16[1024,512]{1,0:T(8,128)(2,1)} %param.26) | copy-start | bytes 3145732
  6.5 70.8 %copy-start.4 = (bf16[1024,512]{1,0:T(8,128)(2,1)S(1)}, bf16[1024,512]{1,0:T(8,128)(2,1)}, u32[]{:S(2)}) copy-start(bf16[1024,512]{1,0:T(8,128)(2,1)} %param.27) | copy-start | bytes 3145732
  6.5 125.2 %all-gather.4.cloned.1.call-start = ((), (), s32[]{:S(2)}) async-start(), calls=%async_computation.1 | async-start | bytes 2621440 | tf_op jit(solution)/shard_map/all_gather | solution.py:101
  7.3 128.2 %all-gather.6.cloned.1.call-start = ((), (), s32[]{:S(2)}) async-start(), calls=%async_computation.2 | async-start | bytes 2621440 | tf_op jit(solution)/shard_map/all_gather | solution.py:102
  8.0 208.6 %all-gather.8.cloned.1.call-start = ((), (), s32[]{:S(2)}) async-start(), calls=%async_computation.3 | async-start | bytes 5242880 | tf_op jit(solution)/shard_map/all_gather | solution.py:173
  8.1 70.5 %collective-permute-start.2 = (bf16[512,512]{1,0:T(8,128)(2,1)}, bf16[512,512]{1,0:T(8,128)(2,1)S(1)}, u32[]{:S(2)}, u32[]{:S(2)}) collective-permute-start(bf16[512,512]{1,0:T(8,128)(2,1)} %param.16), channel_id=1, source_target_pairs={{0,8},{8,16},{16,24},{24,0},{1,9},{9,17},{17,25},{25,1},{2,10},{10... | collective-permute-start | bytes 1572872 | tf_op jit(solution)/shard_map/ppermute | solution.py:23
  72.7 8.6 %copy-start.6 = (f32[31,512]{1,0:T(8,128)S(1)}, f32[31,512]{1,0:T(8,128)}, u32[]{:S(2)}) copy-start(f32[31,512]{1,0:T(8,128)} %param.22) | copy-start | bytes 190468
  73.1 33.4 %collective-permute-start = (bf16[128,256]{0,1:T(8,128)(2,1)S(1)}, bf16[128,256]{0,1:T(8,128)(2,1)S(1)}, u32[]{:S(2)}, u32[]{:S(2)}) collective-permute-start(bf16[128,256]{0,1:T(8,128)(2,1)S(1)} %get-tuple-element.21), channel_id=1, source_target_pairs={{0,8},{8,16},{16,24},{1,9},{9,17},{17,25},{2,10},{10,18},{18,26},{... | collective-permute-start | bytes 196616 | tf_op jit(solution)/shard_map/ppermute | solution.py:36
  76.0 30.4 %collective-permute-start.1 = (bf16[128,256]{0,1:T(8,128)(2,1)S(1)}, bf16[128,256]{0,1:T(8,128)(2,1)}, u32[]{:S(2)}, u32[]{:S(2)}) collective-permute-start(bf16[128,256]{0,1:T(8,128)(2,1)S(1)} %get-tuple-element.22), channel_id=1, source_target_pairs={{8,0},{16,8},{24,16},{9,1},{17,9},{25,17},{10,2},{18,10},{26,18},{... | collective-permute-start | bytes 196616 | tf_op jit(solution)/shard_map/ppermute | solution.py:39
  77.4 49.0 %copy-start.2 = (bf16[512,512]{1,0:T(8,128)(2,1)S(1)}, bf16[512,512]{1,0:T(8,128)(2,1)}, u32[]{:S(2)}) copy-start(bf16[512,512]{1,0:T(8,128)(2,1)} %param.16) | copy-start | bytes 1572868
  78.5 149.6 %reduce-scatter.2.cloned.1.call-start = ((), (), s32[]{:S(2)}) async-start(), calls=%async_computation.4 | async-start | bytes 1572864 | tf_op jit(solution)/shard_map/reduce_scatter | solution.py:174
  78.6 20.7 %collective-permute-start.3 = (bf16[512,512]{1,0:T(8,128)(2,1)S(1)}, bf16[512,512]{1,0:T(8,128)(2,1)S(1)}, u32[]{:S(2)}, u32[]{:S(2)}) collective-permute-start(bf16[512,512]{1,0:T(8,128)(2,1)S(1)} %collective-permute-done.2), channel_id=1, source_target_pairs={{0,8},{8,16},{16,24},{24,0},{1,9},{9,17},{17,25},{25,1},{2,10},{10... | collective-permute-start | bytes 1572872 | tf_op jit(solution)/shard_map/ppermute | solution.py:23
  99.3 27.0 %collective-permute-start.4 = (bf16[512,512]{1,0:T(8,128)(2,1)S(1)}, bf16[512,512]{1,0:T(8,128)(2,1)S(1)}, u32[]{:S(2)}, u32[]{:S(2)}) collective-permute-start(bf16[512,512]{1,0:T(8,128)(2,1)S(1)} %collective-permute-done.3), channel_id=1, source_target_pairs={{0,8},{8,16},{16,24},{24,0},{1,9},{9,17},{17,25},{25,1},{2,10},{10... | collective-permute-start | bytes 1572872 | tf_op jit(solution)/shard_map/ppermute | solution.py:23
  107.3 19.3 %copy-start.3 = (bf16[256,2048]{1,0:T(8,128)(2,1)S(1)}, bf16[256,2048]{1,0:T(8,128)(2,1)}, u32[]{:S(2)}) copy-start(bf16[256,2048]{1,0:T(8,128)(2,1)} %param.14) | copy-start | bytes 3145732
  107.3 19.3 %copy-start.39 = (f32[256]{0:T(256)S(1)}, f32[256]{0:T(256)}, u32[]{:S(2)}) copy-start(f32[256]{0:T(256)} %copy-done.38) | copy-start | bytes 3076
  107.4 19.3 %copy-start.41 = (f32[2048]{0:T(1024)S(1)}, f32[2048]{0:T(1024)}, u32[]{:S(2)}) copy-start(f32[2048]{0:T(1024)} %param.15) | copy-start | bytes 24580
  135.4 11.2 %copy-start.1 = (f32[2,512,256,4]{2,1,3,0:T(8,128)S(1)}, f32[2,512,256,4]{2,1,3,0:T(8,128)}, u32[]{:S(2)}) copy-start(f32[2,512,256,4]{2,1,3,0:T(8,128)} %copy-done) | copy-start | bytes 12582916
  139.3 9.1 %collective-permute-start.5 = (bf16[15,512]{1,0:T(8,128)(2,1)S(1)}, bf16[15,512]{1,0:T(8,128)(2,1)S(1)}, u32[]{:S(2)}, u32[]{:S(2)}) collective-permute-start(bf16[15,512]{1,0:T(8,128)(2,1)S(1)} %get-tuple-element.15), channel_id=1, source_target_pairs={{0,8},{8,16},{16,24},{1,9},{9,17},{17,25},{2,10},{10,18},{18,26},{... | collective-permute-start | bytes 46088 | tf_op jit(solution)/shard_map/ppermute | solution.py:36
  145.3 9.1 %collective-permute-start.6 = (bf16[15,512]{1,0:T(8,128)(2,1)S(1)}, bf16[15,512]{1,0:T(8,128)(2,1)S(1)}, u32[]{:S(2)}, u32[]{:S(2)}) collective-permute-start(bf16[15,512]{1,0:T(8,128)(2,1)S(1)} %get-tuple-element.16), channel_id=1, source_target_pairs={{8,0},{16,8},{24,16},{9,1},{17,9},{25,17},{10,2},{18,10},{26,18},{... | collective-permute-start | bytes 46088 | tf_op jit(solution)/shard_map/ppermute | solution.py:39
  146.6 7.8 %copy-start.7 = (f32[1,512]{1,0:T(1,128)S(1)}, f32[1,512]{1,0:T(1,128)}, u32[]{:S(2)}) copy-start(f32[1,512]{1,0:T(1,128)} %get-tuple-element.29) | copy-start | bytes 6148
  146.6 7.8 %copy-start.8 = (f32[1,512]{1,0:T(1,128)S(1)}, f32[1,512]{1,0:T(1,128)}, u32[]{:S(2)}) copy-start(f32[1,512]{1,0:T(1,128)} %get-tuple-element.30) | copy-start | bytes 6148
  146.6 7.8 %copy-start.9 = (f32[1,512]{1,0:T(1,128)S(1)}, f32[1,512]{1,0:T(1,128)}, u32[]{:S(2)}) copy-start(f32[1,512]{1,0:T(1,128)} %get-tuple-element.31) | copy-start | bytes 6148
  146.7 7.8 %copy-start.10 = (f32[1,512]{1,0:T(1,128)S(1)}, f32[1,512]{1,0:T(1,128)}, u32[]{:S(2)}) copy-start(f32[1,512]{1,0:T(1,128)} %get-tuple-element.32) | copy-start | bytes 6148
  146.7 7.8 %copy-start.11 = (f32[1,512]{1,0:T(1,128)S(1)}, f32[1,512]{1,0:T(1,128)}, u32[]{:S(2)}) copy-start(f32[1,512]{1,0:T(1,128)} %get-tuple-element.33) | copy-start | bytes 6148
  146.7 7.8 %copy-start.12 = (f32[1,512]{1,0:T(1,128)S(1)}, f32[1,512]{1,0:T(1,128)}, u32[]{:S(2)}) copy-start(f32[1,512]{1,0:T(1,128)} %get-tuple-element.34) | copy-start | bytes 6148
  146.7 7.8 %copy-start.13 = (f32[1,512]{1,0:T(1,128)S(1)}, f32[1,512]{1,0:T(1,128)}, u32[]{:S(2)}) copy-start(f32[1,512]{1,0:T(1,128)} %get-tuple-element.35) | copy-start | bytes 6148
  146.7 7.8 %copy-start.14 = (f32[1,512]{1,0:T(1,128)S(1)}, f32[1,512]{1,0:T(1,128)}, u32[]{:S(2)}) copy-start(f32[1,512]{1,0:T(1,128)} %get-tuple-element.36) | copy-start | bytes 6148
  146.7 7.8 %copy-start.15 = (f32[1,512]{1,0:T(1,128)S(1)}, f32[1,512]{1,0:T(1,128)}, u32[]{:S(2)}) copy-start(f32[1,512]{1,0:T(1,128)} %get-tuple-element.37) | copy-start | bytes 6148
  146.7 7.8 %copy-start.16 = (f32[1,512]{1,0:T(1,128)S(1)}, f32[1,512]{1,0:T(1,128)}, u32[]{:S(2)}) copy-start(f32[1,512]{1,0:T(1,128)} %get-tuple-element.38) | copy-start | bytes 6148
  146.7 7.8 %copy-start.17 = (f32[1,512]{1,0:T(1,128)S(1)}, f32[1,512]{1,0:T(1,128)}, u32[]{:S(2)}) copy-start(f32[1,512]{1,0:T(1,128)} %get-tuple-element.39) | copy-start | bytes 6148
  146.9 16.0 %copy-start.36 = (f32[512]{0:T(512)S(1)}, f32[512]{0:T(512)}, u32[]{:S(2)}) copy-start(f32[512]{0:T(512)} %param.25) | copy-start | bytes 6148
  146.9 16.0 %copy-start.37 = (f32[512]{0:T(512)S(1)}, f32[512]{0:T(512)}, u32[]{:S(2)}) copy-start(f32[512]{0:T(512)} %param.24) | copy-start | bytes 6148
  (22 other events, 152.2 us)
Sparse Core Ops, SparseCore 0:
  8.9 68.2 all-gather.3
  78.8 56.6 all-gather.5
  137.0 79.6 all-gather.7
  221.2 6.8 reduce-scatter.1
